TPU v7x, 128 devices: a whole 4x4x4 slice. The times are simulated.
128 devices in a mesh: ep: 16 (over z, x), tp: 8 (over y, core).
Axes of the slice: x: 4, y: 4, z: 4, core: 2. Of those that a mesh axis runs over, the one named last changes fastest.
Arguments:
- mixer_rows: bfloat16 [4096, 4096], P('ep'), may hold values from -8 to 8, as said below
- mixer_gain: float32 [4096], replicated, may hold values from 0.1 to 1.9
- gate_proj: bfloat16 [4096, 4096], P(None, 'tp'), may hold values from -0.09375 to 0.09375
- input_proj: bfloat16 [4096, 4096], P(None, 'tp'), may hold values from -0.09375 to 0.09375
- conv_taps: float32 [4, 4096], P(None, 'tp'), may hold values from -2 to 2
- input_gates: bfloat16 [16, 256, 256], P('tp'), may hold values from -0.375 to 0.375
- decay_gates: bfloat16 [16, 256, 256], P('tp'), may hold values from -0.375 to 0.375
- decay_offset: float32 [4096], P('tp'), may hold values from 4.8 to 13, as said below
- out_proj: bfloat16 [4096, 4096], P('tp'), may hold values from -0.09375 to 0.09375
- mixer_scale: float32 [4096], replicated, may hold values from 0.1 to 1.9
- expert_rows: bfloat16 [4096, 4096], P('ep'), may hold values from -6 to 6
- expert_gain: float32 [4096], replicated, may hold values from 0.1 to 1.9
- route_ids: int32 [4096, 2], P('ep'), may hold values from 0 to 15, all different within a row; in each aligned block of 256 rows (0 to 255, 256 to 511, ...) at most 48 rows name the same one
- route_weights: float32 [4096, 2], P('ep'), may hold values from 0.5 to 2
- expert_gate: bfloat16 [16, 4096, 1024], P('ep', None, 'tp'), may hold values from -0.09375 to 0.09375
- expert_up: bfloat16 [16, 4096, 1024], P('ep', None, 'tp'), may hold values from -0.09375 to 0.09375
- expert_down: bfloat16 [16, 1024, 4096], P('ep', 'tp'), may hold values from -0.1875 to 0.1875
- shared_gate: bfloat16 [4096, 1024], P(None, 'tp'), may hold values from -0.09375 to 0.09375
- shared_up: bfloat16 [4096, 1024], P(None, 'tp'), may hold values from -0.09375 to 0.09375
- shared_down: bfloat16 [1024, 4096], P('tp'), may hold values from -0.1875 to 0.1875
- expert_scale: float32 [4096], replicated, may hold values from 0.1 to 1.9
Outputs:
- mixer_out: bfloat16 [4096, 4096], P(('ep', 'tp'))
- expert_out: bfloat16 [4096, 4096], P(('ep', 'tp'))
Inputs may be any that keep to these rules, and one draw needn't show every extreme that they name: `mixer_rows`: order one, with a common direction whose weight drifts slowly along the sequence. `decay_offset`: the even channels forget within some 30 to 200 tokens; the odd channels keep 5 to 90 percent of their state over the whole sequence of 4096 tokens. `route_ids`: each row names 2 different experts; within the rows of one index of ep (aligned blocks of 256 rows) no expert is named by more than 48 rows, and in some blocks one is named by exactly 48.
All inputs are finite; a program needn't handle non-finite values.
Results may differ from a plain program's by a relative error of at most 0.0033.
The roundings to bfloat16 on the way count: a program that leaves them out, or rounds other values in their place, can miss the bound.
Values may be sent and summed in bfloat16 or wider, within the bound.
A program may use at most 192 MiB of HBM per device.

v0:
```python
import jax
import jax.numpy as jnp
from jax import lax
from jax.sharding import PartitionSpec as P

eps = 1e-06
lru_power = 8.0


def shifted(block, axis, distance):
    devices = range(lax.axis_size(axis))
    route = [(i - distance, i) for i in devices if i - distance in devices]
    return lax.ppermute(block, axis, route)


def sent_to_all(shard, axis):
    length = lax.axis_size(axis)
    return lax.all_to_all(
        jnp.broadcast_to(shard[None], (length, *shard.shape)), axis, 0, 0, tiled=True
    )


def collected_together(shard, axis):
    leaves = jax.tree.leaves(shard)
    turns = sorted(range(len(leaves)), key=lambda k: -leaves[k].size)
    width = (1, *leaves[turns[0]].shape)[-1]
    lines = [
        jnp.pad(leaves[k].reshape(-1), (0, -leaves[k].size % width)).reshape(-1, width)
        for k in turns
    ]
    both, at, found = (sent_to_all(jnp.concatenate(lines), axis), 0, {})
    for k, line in zip(turns, lines):
        share = both[:, at : at + len(line)].reshape(len(both), -1)
        found[k] = share[:, : leaves[k].size].reshape(-1, *leaves[k].shape)
        at += len(line)
    numbers = iter(range(len(leaves)))
    return jax.tree.map(lambda _: found[next(numbers)], shard)


def folded_in_pairs(pieces, combine):
    while len(jax.tree.leaves(pieces)[0]) > 1:
        pieces = jax.vmap(combine)(
            *(jax.tree.map(lambda part: part[side::2], pieces) for side in (0, 1))
        )
    return jax.tree.map(lambda part: part[0], pieces)


def carried_in(shard, axis, combine, identity):
    length, mine = (lax.axis_size(axis), lax.axis_index(axis))
    passed = jnp.arange(length) < mine

    def kept(part, zero, own):
        part = jnp.where(
            passed.reshape(-1, *(1 for _ in own.shape)), part, jnp.asarray(zero, own.dtype)
        )
        return part

    pieces = collected_together(shard, axis)
    return folded_in_pairs(jax.tree.map(kept, pieces, identity, shard), combine)


def sent_together(arrays, axis, dim, along):
    both = jnp.concatenate(arrays, axis=along)
    whole, at, outs = (lax.psum_scatter(both, axis, scatter_dimension=dim, tiled=True), 0, [])
    for a in arrays:
        outs.append(lax.slice_in_dim(whole, at, at + a.shape[along], axis=along))
        at += a.shape[along]
    return tuple(outs)


def rms_scale(values, scale):
    floats = values.astype(jnp.float32)
    return floats * lax.rsqrt(jnp.mean(floats * floats, axis=-1, keepdims=True) + eps) * scale


def linear_pair(earlier, later):
    return (earlier[0] * later[0], later[0] * earlier[1] + later[1])


def slot_table(route_ids, expert_count, capacity):
    id_list = route_ids.reshape(-1)
    indicator = (id_list[:, None] == jnp.arange(expert_count, dtype=jnp.int32)[None, :]).astype(
        jnp.int32
    )
    earlier_count = jnp.cumsum(indicator, axis=0) - indicator
    position = jnp.sum(earlier_count * indicator, axis=1)
    slot_ids = id_list * capacity + position
    matched = (
        slot_ids[None, :] == jnp.arange(expert_count * capacity, dtype=jnp.int32)[:, None]
    ).astype(jnp.int32)
    source = jnp.sum(matched * jnp.arange(id_list.shape[0], dtype=jnp.int32)[None, :], axis=1)
    filled = jnp.sum(matched, axis=1) > 0
    return (slot_ids, source, filled)


def body(
    mixer_rows,
    mixer_gain,
    gate_proj,
    input_proj,
    conv_taps,
    input_gates,
    decay_gates,
    decay_offset,
    out_proj,
    mixer_scale,
    expert_rows,
    expert_gain,
    route_ids,
    route_weights,
    expert_gate,
    expert_up,
    expert_down,
    shared_gate,
    shared_up,
    shared_down,
    expert_scale,
):
    row_count = mixer_rows.shape[0]
    normed = rms_scale(mixer_rows, mixer_gain).astype(jnp.bfloat16)
    gate_branch = jax.nn.gelu(jnp.dot(normed, gate_proj, preferred_element_type=jnp.float32))
    branch = jnp.dot(normed, input_proj, preferred_element_type=jnp.float32).astype(jnp.bfloat16)
    tap_count = conv_taps.shape[0]
    earlier_rows = shifted(branch[row_count - tap_count + 1 :], "ep", 1)
    padded = jnp.concatenate([earlier_rows, branch], axis=0)
    conv_sum = conv_taps[0] * padded[0:row_count].astype(jnp.float32)
    for tap_index in range(1, tap_count):
        conv_sum = conv_sum + conv_taps[tap_index] * padded[
            tap_index : tap_index + row_count
        ].astype(jnp.float32)
    conv_out = conv_sum.astype(jnp.bfloat16)
    block_rows = conv_out.reshape(row_count, input_gates.shape[0], input_gates.shape[1])
    input_gate = jax.nn.sigmoid(
        jnp.einsum("rbi,bij->rbj", block_rows, input_gates, preferred_element_type=jnp.float32)
    ).reshape(row_count, -1)
    decay_gate = jax.nn.sigmoid(
        jnp.einsum("rbi,bij->rbj", block_rows, decay_gates, preferred_element_type=jnp.float32)
    ).reshape(row_count, -1)
    log_decay = -lru_power * decay_gate * jax.nn.softplus(-decay_offset)
    positions = lax.axis_index("ep") * row_count + jnp.arange(row_count, dtype=jnp.int32)
    input_scale = jnp.where((positions == 0)[:, None], 1.0, jnp.sqrt(-jnp.expm1(2.0 * log_decay)))
    drive_term = input_scale * input_gate * conv_out.astype(jnp.float32)
    decay_rate = jnp.exp(log_decay)
    decay_product, local_states = lax.associative_scan(
        linear_pair, (decay_rate, drive_term), axis=0
    )
    carried = carried_in(
        (decay_product[-1], local_states[-1]),
        "ep",
        linear_pair,
        (jnp.ones_like(decay_rate[0]), jnp.zeros_like(decay_rate[0])),
    )
    states = local_states + decay_product * carried[1][None, :]
    gated_rows = (gate_branch * states).astype(jnp.bfloat16)
    mixer_term = jnp.dot(gated_rows, out_proj, preferred_element_type=jnp.float32)
    ep_size = lax.axis_size("ep")
    local_experts = expert_gate.shape[0]
    expert_count = local_experts * ep_size
    top_count = route_ids.shape[1]
    token_count = expert_rows.shape[0]
    row_width = expert_rows.shape[1]
    capacity = token_count * top_count * 3 // (2 * expert_count)
    expert_normed = rms_scale(expert_rows, expert_gain).astype(jnp.bfloat16)
    slot_ids, source, filled = slot_table(route_ids, expert_count, capacity)
    outgoing = jnp.where(
        filled[:, None], expert_normed[source // top_count], jnp.zeros((), jnp.bfloat16)
    )
    outgoing = outgoing.reshape(ep_size, local_experts, capacity, row_width)
    received = lax.all_to_all(outgoing, "ep", split_axis=0, concat_axis=0, tiled=True)
    gate_part = jnp.einsum(
        "secd,edf->secf", received, expert_gate, preferred_element_type=jnp.float32
    )
    up_part = jnp.einsum("secd,edf->secf", received, expert_up, preferred_element_type=jnp.float32)
    copy_hidden = (jax.nn.silu(gate_part) * up_part).astype(jnp.bfloat16)
    column_sums = lax.psum_scatter(
        jnp.einsum("secf,efd->secd", copy_hidden, expert_down, preferred_element_type=jnp.float32),
        "tp",
        scatter_dimension=3,
        tiled=True,
    )
    result = lax.all_to_all(column_sums, "ep", split_axis=0, concat_axis=0, tiled=True)
    flat_back = result.reshape(expert_count * capacity, -1)
    picked = flat_back[slot_ids] * route_weights.reshape(-1, 1)
    routed = jnp.sum(picked.reshape(token_count, top_count, -1), axis=1)
    shared_hidden = (
        jax.nn.silu(jnp.dot(expert_normed, shared_gate, preferred_element_type=jnp.float32))
        * jnp.dot(expert_normed, shared_up, preferred_element_type=jnp.float32)
    ).astype(jnp.bfloat16)
    shared_term = jnp.dot(shared_hidden, shared_down, preferred_element_type=jnp.float32)
    mixer_sum, expert_sum = sent_together((mixer_term, shared_term), "tp", 0, 1)
    expert_sum = expert_sum + lax.all_to_all(routed, "tp", split_axis=0, concat_axis=1, tiled=True)
    mixer_out = rms_scale(mixer_sum, mixer_scale).astype(jnp.bfloat16)
    expert_out = rms_scale(expert_sum, expert_scale).astype(jnp.bfloat16)
    return (mixer_out, expert_out)


def solution(mesh):
    placed = (
        P("ep", None),
        P(),
        P(None, "tp"),
        P(None, "tp"),
        P(None, "tp"),
        P("tp", None, None),
        P("tp", None, None),
        P("tp"),
        P("tp", None),
        P(),
        P("ep", None),
        P(),
        P("ep", None),
        P("ep", None),
        P("ep", None, "tp"),
        P("ep", None, "tp"),
        P("ep", "tp", None),
        P(None, "tp"),
        P(None, "tp"),
        P("tp", None),
        P(),
    )
    return jax.shard_map(
        body,
        mesh=mesh,
        in_specs=placed,
        out_specs=(P(("ep", "tp"), None), P(("ep", "tp"), None)),
        check_vma=False,
    )
```

profile of v0, /device:TPU:1, one launch (start us, length us, event | category | flops | bytes accessed | tf_op | source)
XLA Modules:
  0.0 264.7 jit_solution(15755040382263902929)
XLA Ops:
  7.2 0.9 copy.64
  8.4 2.1 fusion.7
  10.5 1.2 reduce-window.6
  12.0 0.5 convert_reduce_fusion
  12.7 2.2 fusion.9
  14.9 5.7 %gather_fusion = bf16[768,4096]{1,0:T(8,128)(2,1)} fusion(bf16[256,4096]{1,0:T(8,128)(2,1)S(1)} %fusion.9, s32[1024]{0:T(1024)S(1)} %pad_clamp_fusion.1), kind=kCustom, calls=%fused_computation | custom fusion | bytes 12585984 | tf_op jit(solution)/shard_map/gather | solution.py:166
  20.6 3.3 %broadcast_select_fusion = bf16[16,1,48,4096]{3,2,1,0:T(8,128)(2,1)S(1)} fusion(bf16[16,1,48,4096]{3,2,1,0:T(8,128)(2,1)} %bitcast.125, pred[16,48]{1,0:T(8,128)(4,1)S(1)} %gt.11), kind=kLoop, calls=%fused_computation.8 | loop fusion | flops 3145728 | bytes 12583680 | tf_op jit(solution)/shard_map/jit(_where)/select_n | solution.py:165
  23.9 80.6 %all_to_all.34 = bf16[16,1,48,4096]{3,2,1,0:T(8,128)(2,1)S(1)} all-to-all(bf16[16,1,48,4096]{3,2,1,0:T(8,128)(2,1)S(1)} %broadcast_select_fusion), channel_id=1, replica_groups=mesh['ep'=16,'tp'=8] {'ep'}, dimensions={0} | all-to-all | bytes 12582912 | tf_op jit(solution)/shard_map/all_to_all | solution.py:169
  104.5 2.6 copy-done.2
  107.1 1.8 fusion.16
  108.9 14.1 %convolution_bitcast_fusion = f32[16,1,48,4096]{3,2,0,1:T(8,128)} fusion(bf16[1,128,4096]{2,1,0:T(8,128)(2,1)S(1)} %copy-done, bf16[16,1,48,4096]{3,2,1,0:T(8,128)(2,1)} %copy-done.2, bf16[1,4096,128]{2,1,0:T(8,128)(2,1)} %param.36, f32[16,1,48,128]{3,2,0,1:T(8,128)S(1)} %fusion.16), kind=kOutput, calls=%fused_computation.3 | convolution fusion | flops 1611202560 | bytes 21364736 | tf_op jit(solution)/shard_map/secf,efd->secd/dot_general | solution.py:176
  123.1 2.1 fusion.4
  125.2 4.2 %convolution_convert_fusion = bf16[256,512]{1,0:T(8,128)(2,1)S(1)} fusion(bf16[4096,512]{1,0:T(8,128)(2,1)} %param.24, bf16[256,4096]{1,0:T(8,128)(2,1)} %param.21, f32[4096]{0:T(1024)S(1)} %copy-done.8, f32[256]{0:T(256)S(1)} %add_rsqrt_fusion.1), kind=kOutput, calls=%fused_computation.32 | convolution fusion | flops 1078067200 | bytes 6571008 | tf_op jit(solution)/shard_map/dot_general | solution.py:122
  129.4 0.6 slice.435
  130.0 2.8 %collective-permute-start = (bf16[3,512]{1,0:T(4,128)(2,1)}, bf16[3,512]{1,0:T(4,128)(2,1)}, u32[]{:S(2)}, u32[]{:S(2)}) collective-permute-start(bf16[3,512]{1,0:T(4,128)(2,1)} %slice.435), channel_id=1, source_target_pairs={{0,8},{8,16},{16,24},{24,32},{32,40},{40,48},{48,56},{56,64},{64,7... | collective-permute-start | bytes 9224 | tf_op jit(solution)/shard_map/ppermute | solution.py:13
  132.8 0.6 fusion.104
  133.4 0.6 fusion.115
  134.0 0.7 fusion.117
  134.7 4.9 %fusion.32 = f32[256,4096]{1,0:T(8,128)} fusion(bf16[128,4096]{1,0:T(8,128)(2,1)} %param.40, bf16[256,4096]{1,0:T(8,128)(2,1)S(1)} %fusion.9, bf16[4096,128]{1,0:T(8,128)(2,1)} %param.39, f32[256,128]{1,0:T(8,128)S(1)} %fusion.117), kind=kOutput, calls=%fused_computation.38 | convolution fusion | flops 537067520 | bytes 8519680 | tf_op jit(solution)/shard_map/dot_general | solution.py:189
  139.7 1.0 add_convert_fusion
  140.7 0.4 fusion.13
  141.8 0.4 convert_multiply_fusion.4
  145.4 1.4 slice.335
  146.8 1.4 slice.392
  149.4 1.7 pad.129
  151.3 2.0 fusion.74
  153.3 0.7 pad_maximum_fusion.3
  154.0 1.1 pad.128
  155.1 1.7 pad.113
  156.8 1.0 pad_maximum_fusion.2
  157.8 1.8 pad.112
  159.5 0.7 slice_add_fusion.3
  160.3 0.7 slice_add_fusion.2
  161.0 0.6 broadcast_in_dim.44
  161.7 4.9 %all-to-all-start = ((f32[16,2,512]{2,1,0:T(2,128)}), f32[16,2,512]{2,1,0:T(2,128)S(1)}, u32[]{:S(2)}, u32[]{:S(2)}) async-start(f32[16,2,512]{2,1,0:T(2,128)} %broadcast_in_dim.44), calls=%async_computation | async-start | bytes 131072 | tf_op jit(solution)/shard_map/all_to_all | solution.py:18
  166.6 6.5 %all-to-all-done = f32[16,2,512]{2,1,0:T(2,128)S(1)} async-done(((f32[16,2,512]{2,1,0:T(2,128)}), f32[16,2,512]{2,1,0:T(2,128)S(1)}, u32[]{:S(2)}, u32[]{:S(2)}) %all-to-all-start) | async-done | bytes 65568 | tf_op jit(solution)/shard_map/all_to_all | solution.py:18
  173.5 8.6 %fusion.59 = f32[256,4096]{1,0:T(8,128)} fusion(bf16[512,4096]{1,0:T(8,128)(2,1)} %param.29, bf16[4096,512]{1,0:T(8,128)(2,1)} %param.23, bf16[256,4096]{1,0:T(8,128)(2,1)S(1)} %copy-done.3, f32[4096]{0:T(1024)S(1)} %copy-done.9, f32[256]{0:T(256)S(1)} %copy-done.15, f32[256,512]{1,0:T(8,128)S(1)} %pad.128, f32[256,512]{1,0:T(8,128)S(1)} %copy-done.4, ...), kind=kOutput, calls=%fused_computation.54 | convolution fusion | flops 2153512960 | bytes 16796672 | tf_op jit(solution)/shard_map/dot_general | solution.py:155
  182.1 7.7 %pad_maximum_fusion = f32[256,8192]{1,0:T(8,128)} fusion(f32[256,4096]{1,0:T(8,128)} %fusion.32, f32[256,4096]{1,0:T(8,128)} %fusion.59), kind=kLoop, calls=%fused_computation.2 | loop fusion | flops 2097152 | bytes 16777216 | tf_op jit(solution)/shard_map/concatenate | solution.py:63
  189.9 4.3 %reduce-scatter.5.cloned.1.call-done = f32[16,1,48,512]{3,2,0,1:T(8,128)} async-done(((f32[16,1,48,4096]{3,2,0,1:T(8,128)}), f32[16,1,48,512]{3,2,0,1:T(8,128)}) %reduce-scatter.5.cloned.1.call-update) | async-done | bytes 1572880 | tf_op jit(solution)/shard_map/reduce_scatter | solution.py:175
  194.1 6.7 %all-to-all-start.2 = ((f32[16,1,48,512]{3,2,1,0:T(8,128)}), f32[16,1,48,512]{3,2,1,0:T(8,128)S(1)}, u32[]{:S(2)}, u32[]{:S(2)}) async-start(f32[16,1,48,512]{3,2,1,0:T(8,128)} %bitcast.130), calls=%async_computation.4 | async-start | bytes 3145728 | tf_op jit(solution)/shard_map/all_to_all | solution.py:181
  201.3 20.8 %all-to-all-done.2 = f32[16,1,48,512]{3,2,1,0:T(8,128)S(1)} async-done(((f32[16,1,48,512]{3,2,1,0:T(8,128)}), f32[16,1,48,512]{3,2,1,0:T(8,128)S(1)}, u32[]{:S(2)}, u32[]{:S(2)}) %all-to-all-start.2) | async-done | bytes 1572896 | tf_op jit(solution)/shard_map/all_to_all | solution.py:181
  222.1 2.3 gather_fusion.1
  224.4 2.0 gather.13
  226.4 1.3 multiply_reduce_fusion
  227.7 22.3 %all_to_all.35 = f32[8,32,512]{2,1,0:T(8,128)S(1)} all-to-all(f32[8,32,512]{2,1,0:T(8,128)S(1)} %bitcast.128), channel_id=1, replica_groups=mesh['ep'=16,'tp'=8] {'tp'}, dimensions={0} | all-to-all | bytes 1048576 | tf_op jit(solution)/shard_map/all_to_all | solution.py:191
  250.1 4.2 %reduce-scatter.3.cloned.1.call-done = f32[32,8192]{1,0:T(8,128)} async-done(((f32[256,8192]{1,0:T(8,128)}), f32[32,8192]{1,0:T(8,128)}) %reduce-scatter.3.cloned.1.call-update) | async-done | bytes 1048592 | tf_op jit(solution)/shard_map/reduce_scatter | solution.py:64
  254.3 1.4 multiply_reduce_fusion.1
  255.7 2.2 multiply_convert_fusion
  (205 shorter events, 6.5 us)
Async XLA Ops:
  7.2 101.7 %copy-start = (bf16[1,128,4096]{2,1,0:T(8,128)(2,1)S(1)}, bf16[1,128,4096]{2,1,0:T(8,128)(2,1)}, u32[]{:S(2)}) copy-start(bf16[1,128,4096]{2,1,0:T(8,128)(2,1)} %param.37) | copy-start | bytes 3145732
  7.2 187.0 %reduce-scatter.5.cloned.1.call-start = ((), (), s32[]{:S(2)}) async-start(), calls=%async_computation.7 | async-start | bytes 14155776 | tf_op jit(solution)/shard_map/reduce_scatter | solution.py:175
  23.9 83.2 %copy-start.18 = (bf16[1,4096,128]{2,1,0:T(8,128)(2,1)S(1)}, bf16[1,4096,128]{2,1,0:T(8,128)(2,1)}, u32[]{:S(2)}) copy-start(bf16[1,4096,128]{2,1,0:T(8,128)(2,1)} %param.35) | copy-start | bytes 3145732
  104.5 2.6 copy-start.2
  123.0 2.1 copy-start.8
  125.2 4.3 %copy-start.14 = (f32[256]{0:T(256)}, f32[256]{0:T(256)S(1)}, u32[]{:S(2)}) copy-start(f32[256]{0:T(256)S(1)} %add_rsqrt_fusion.1) | copy-start | bytes 3076
  125.2 7.6 %copy-start.17 = (f32[512]{0:T(512)S(1)}, f32[512]{0:T(512)}, u32[]{:S(2)}) copy-start(f32[512]{0:T(512)} %param.28) | copy-start | bytes 6148
  125.2 8.2 %copy-start.12 = (f32[4,512]{1,0:T(4,128)S(1)}, f32[4,512]{1,0:T(4,128)}, u32[]{:S(2)}) copy-start(f32[4,512]{1,0:T(4,128)} %param.25) | copy-start | bytes 24580
  125.2 8.8 %copy-start.5 = (bf16[4096,128]{1,0:T(8,128)(2,1)S(1)}, bf16[4096,128]{1,0:T(8,128)(2,1)}, u32[]{:S(2)}) copy-start(bf16[4096,128]{1,0:T(8,128)(2,1)} %param.38) | copy-start | bytes 3145732
  130.0 9.6 %collective-permute-start = (bf16[3,512]{1,0:T(4,128)(2,1)}, bf16[3,512]{1,0:T(4,128)(2,1)}, u32[]{:S(2)}, u32[]{:S(2)}) collective-permute-start(bf16[3,512]{1,0:T(4,128)(2,1)} %slice.435), channel_id=1, source_target_pairs={{0,8},{8,16},{16,24},{24,32},{32,40},{40,48},{48,56},{56,64},{64,7... | collective-permute-start | bytes 9224 | tf_op jit(solution)/shard_map/ppermute | solution.py:13
  134.7 4.9 %copy-start.11 = (f32[1,512]{1,0:T(1,128)S(1)}, f32[1,512]{1,0:T(1,128)}, u32[]{:S(2)}) copy-start(f32[1,512]{1,0:T(1,128)} %get-tuple-element.47) | copy-start | bytes 6148
  134.7 6.0 %copy-start.19 = (bf16[2,256,256]{2,1,0:T(8,128)(2,1)S(1)}, bf16[2,256,256]{2,1,0:T(8,128)(2,1)}, u32[]{:S(2)}) copy-start(bf16[2,256,256]{2,1,0:T(8,128)(2,1)} %param.27) | copy-start | bytes 786436
  139.6 1.6 copy-start.20
  139.6 2.2 copy-start.13
  151.1 22.4 %copy-start.3 = (bf16[256,4096]{1,0:T(8,128)(2,1)S(1)}, bf16[256,4096]{1,0:T(8,128)(2,1)}, u32[]{:S(2)}) copy-start(bf16[256,4096]{1,0:T(8,128)(2,1)} %param.21) | copy-start | bytes 6291460
  151.1 22.4 %copy-start.9 = (f32[4096]{0:T(1024)S(1)}, f32[4096]{0:T(1024)}, u32[]{:S(2)}) copy-start(f32[4096]{0:T(1024)} %param.22) | copy-start | bytes 49156
  151.1 22.4 %copy-start.15 = (f32[256]{0:T(256)S(1)}, f32[256]{0:T(256)}, u32[]{:S(2)}) copy-start(f32[256]{0:T(256)} %copy-done.14) | copy-start | bytes 3076
  153.3 20.2 %copy-start.4 = (f32[256,512]{1,0:T(8,128)S(1)}, f32[256,512]{1,0:T(8,128)}, u32[]{:S(2)}) copy-start(f32[256,512]{1,0:T(8,128)} %pad.129) | copy-start | bytes 1572868
  161.7 11.4 %all-to-all-start = ((f32[16,2,512]{2,1,0:T(2,128)}), f32[16,2,512]{2,1,0:T(2,128)S(1)}, u32[]{:S(2)}, u32[]{:S(2)}) async-start(f32[16,2,512]{2,1,0:T(2,128)} %broadcast_in_dim.44), calls=%async_computation | async-start | bytes 131072 | tf_op jit(solution)/shard_map/all_to_all | solution.py:18
  166.5 87.7 %reduce-scatter.3.cloned.1.call-start = ((), (), s32[]{:S(2)}) async-start(), calls=%async_computation.6 | async-start | bytes 9437184 | tf_op jit(solution)/shard_map/reduce_scatter | solution.py:64
  189.8 11.0 %copy-start.10 = (s32[256,2]{0,1:T(2,128)S(1)}, s32[256,2]{0,1:T(2,128)}, u32[]{:S(2)}) copy-start(s32[256,2]{0,1:T(2,128)} %param.33) | copy-start | bytes 6148
  189.8 11.3 %copy-start.16 = (f32[256,2]{0,1:T(2,128)S(1)}, f32[256,2]{0,1:T(2,128)}, u32[]{:S(2)}) copy-start(f32[256,2]{0,1:T(2,128)} %param.34) | copy-start | bytes 6148
  194.1 27.9 %all-to-all-start.2 = ((f32[16,1,48,512]{3,2,1,0:T(8,128)}), f32[16,1,48,512]{3,2,1,0:T(8,128)S(1)}, u32[]{:S(2)}, u32[]{:S(2)}) async-start(f32[16,1,48,512]{3,2,1,0:T(8,128)} %bitcast.130), calls=%async_computation.4 | async-start | bytes 3145728 | tf_op jit(solution)/shard_map/all_to_all | solution.py:181
  224.4 31.3 %copy-start.6 = (f32[4096]{0:T(1024)S(1)}, f32[4096]{0:T(1024)}, u32[]{:S(2)}) copy-start(f32[4096]{0:T(1024)} %param.41) | copy-start | bytes 49156
  224.4 31.3 %copy-start.7 = (f32[4096]{0:T(1024)S(1)}, f32[4096]{0:T(1024)}, u32[]{:S(2)}) copy-start(f32[4096]{0:T(1024)} %param.30) | copy-start | bytes 49156
  224.4 33.5 %copy-start.1 = (bf16[1,128,4096]{2,1,0:T(8,128)(2,1)S(1)}, bf16[1,128,4096]{2,1,0:T(8,128)(2,1)}, u32[]{:S(2)}) copy-start(bf16[1,128,4096]{2,1,0:T(8,128)(2,1)} %param.37) | copy-start | bytes 3145732
Sparse Core Ops, SparseCore 0:
  123.2 70.9 reduce-scatter.4
  196.5 57.6 reduce-scatter.2
where the time goes:
time: 265 us
  blocking collectives  103 us (39%)
  waiting for transfers between devices  35.7 us (13%)
  matrix products  35 us (13%)
  other arithmetic  32.2 us (12%)
  local copies, waits for them, and re-layouts  29.4 us (11%)
  between operations  15.1 us (6%)
  starting transfers between devices  14.4 us (5%)
    all_to_all x1, blocking collectives, body(): lax.all_to_all(outgoing, 'ep', split_axis=0, concat_axis=0, tiled=True)  80.6 us
    all_to_all x1, blocking collectives, body(): lax.all_to_all(routed, 'tp', split_axis=0, concat_axis=1, tiled=True)  22.3 us
    all_to_all x1, waiting for transfers between devices, body(): lax.all_to_all(column_sums, 'ep', split_axis=0, concat_axis=0, tiled=True)  20.8 us
    dot_general x1, matrix products, body(): jnp.einsum('secf,efd->secd', copy_hidden, expert_down, preferred_element_...  14.1 us
    dot_general x1, matrix products, body(): jnp.dot(gated_rows, out_proj, preferred_element_type=jnp.float32)  8.58 us
    concatenate x1, other arithmetic, sent_together(): both = jnp.concatenate(arrays, axis=along)  7.72 us
    all_to_all x1, starting transfers between devices, body(): lax.all_to_all(column_sums, 'ep', split_axis=0, concat_axis=0, tiled=True)  6.68 us
    pad x28, local copies, waits for them, and re-layouts, body(): lax.associative_scan(linear_pair, (decay_rate, drive_term), axis=0)  6.67 us
  transfers between devices with their start and end apart: 5, of which 4 were waited for; matrix products, arithmetic and copies ran while one was open for 22% of the time, Pallas kernels for 0%

commit v1 on v0

--- a/solution.py
+++ b/solution.py
@@ -5,6 +5,29 @@
 
 eps = 1e-06
 lru_power = 8.0
+
+
+def cut_along(array, dim, size):
+    lengths = array.shape
+    tiles = array.reshape(*lengths[:dim], size, lengths[dim] // size, *lengths[dim + 1 :])
+    return jnp.moveaxis(tiles, dim, 0)
+
+
+def in_order(pieces, dim):
+    pieces = jnp.moveaxis(pieces, 0, dim)
+    shape = pieces.shape
+    return pieces.reshape(*shape[:dim], shape[dim] * shape[dim + 1], *shape[dim + 2 :])
+
+
+def sent_to_each(x, axis, split_dim, concat_dim):
+    size, mine = (lax.axis_size(axis), lax.axis_index(axis))
+    blocks = cut_along(x, split_dim, size)
+    gathered = [blocks[mine]]
+    for lap in range(1, size):
+        sent = blocks[(mine + lap) % size]
+        gathered.append(lax.ppermute(sent, axis, [(i, (i + lap) % size) for i in range(size)]))
+    blocks = jnp.stack(gathered)[(mine - jnp.arange(size)) % size]
+    return in_order(blocks, concat_dim)
 
 
 def shifted(block, axis, distance):
@@ -178,7 +201,7 @@
         scatter_dimension=3,
         tiled=True,
     )
-    result = lax.all_to_all(column_sums, "ep", split_axis=0, concat_axis=0, tiled=True)
+    result = sent_to_each(column_sums, "ep", 0, 0)
     flat_back = result.reshape(expert_count * capacity, -1)
     picked = flat_back[slot_ids] * route_weights.reshape(-1, 1)
     routed = jnp.sum(picked.reshape(token_count, top_count, -1), axis=1)

time: 265 us -> 268 us (1.011)
  starting transfers between devices: 14.4 us -> 36.3 us
  waiting for transfers between devices: 35.7 us -> 17.5 us
  blocking collectives: 103 us -> 99.7 us
  local copies, waits for them, and re-layouts: 29.4 us -> 32.6 us
    ppermute x0 -> x15, starting transfers between devices: none -> 28.5 us  [sent_to_each(): lax.ppermute(sent, axis, [(i, (i + lap) % size) for i in range(size)])]
    all_to_all x1 -> x0, waiting for transfers between devices: 20.8 us -> none  [body(): lax.all_to_all(column_sums, 'ep', split_axis=0, concat_axis=0, tiled=True)]
    all_to_all x1 -> x0, starting transfers between devices: 6.68 us -> none  [body(): lax.all_to_all(column_sums, 'ep', split_axis=0, concat_axis=0, tiled=True)]
    reduce_scatter x1, waiting for transfers between devices: 4.21 us -> 0.02 us  [sent_together(): lax.psum_scatter(both, axis, scatter_dimension=dim, tiled=True)]
    ppermute x0 -> x15, waiting for transfers between devices: none -> 3.41 us  [sent_to_each(): lax.ppermute(sent, axis, [(i, (i + lap) % size) for i in range(size)])]
    reduce_scatter x1, waiting for transfers between devices: 4.28 us -> 7.53 us  [body(): lax.psum_scatter(jnp.einsum('secf,efd->secd', copy_hidden, expert_down, p...]
    all_to_all x1, blocking collectives: 22.3 us -> 19.1 us  [body(): lax.all_to_all(routed, 'tp', split_axis=0, concat_axis=1, tiled=True)]
    unnamed x44 -> x71, local copies, waits for them, and re-layouts: 3.72 us -> 6.49 us
  transfers between devices with their start and end apart: 5 -> 19, of which waited for: 4 -> 6; matrix products, arithmetic and copies ran while one was open for 22% -> 21% of each run, Pallas kernels for 0% -> 0%
where the time goes in v1:
time: 268 us; the launch traced here: 267 us
  blocking collectives  99.7 us (37%)
  starting transfers between devices  36.3 us (14%)
  matrix products  34.4 us (13%)
  local copies, waits for them, and re-layouts  32.6 us (12%)
  other arithmetic  30.7 us (11%)
  waiting for transfers between devices  17.5 us (7%)
  between operations  15.7 us (6%)
    all_to_all x1, blocking collectives, body(): lax.all_to_all(outgoing, 'ep', split_axis=0, concat_axis=0, tiled=True)  80.6 us
    ppermute x15, starting transfers between devices, sent_to_each(): lax.ppermute(sent, axis, [(i, (i + lap) % size) for i in range(size)])  28.5 us
    all_to_all x1, blocking collectives, body(): lax.all_to_all(routed, 'tp', split_axis=0, concat_axis=1, tiled=True)  19.1 us
    dot_general x1, matrix products, body(): jnp.einsum('secf,efd->secd', copy_hidden, expert_down, preferred_element_...  14.1 us
    dot_general x1, matrix products, body(): jnp.dot(gated_rows, out_proj, preferred_element_type=jnp.float32)  8.59 us
    concatenate x1, other arithmetic, sent_together(): both = jnp.concatenate(arrays, axis=along)  7.74 us
    reduce_scatter x1, waiting for transfers between devices, body(): lax.psum_scatter(jnp.einsum('secf,efd->secd', copy_hidden, expert_down, p...  7.53 us
    pad x28, local copies, waits for them, and re-layouts, body(): lax.associative_scan(linear_pair, (decay_rate, drive_term), axis=0)  6.69 us
  transfers between devices with their start and end apart: 19, of which 6 were waited for; matrix products, arithmetic and copies ran while one was open for 21% of the time, Pallas kernels for 0%

profile of v1, /device:TPU:1, one launch (start us, length us, event | category | flops | bytes accessed | tf_op | source)
XLA Modules:
  0.0 266.8 jit_solution(2413345070313781310)
XLA Ops:
  9.1 2.1 fusion.7
  11.2 1.2 reduce-window.6
  13.7 2.2 fusion.9
  16.5 5.8 %gather_fusion = bf16[768,4096]{1,0:T(8,128)(2,1)} fusion(bf16[256,4096]{1,0:T(8,128)(2,1)S(1)} %fusion.9, s32[1024]{0:T(1024)S(1)} %get-tuple-element.71), kind=kCustom, calls=%fused_computation | custom fusion | bytes 12585984 | tf_op jit(solution)/shard_map/gather | solution.py:189
  22.3 3.3 %broadcast_select_fusion = bf16[16,1,48,4096]{3,2,1,0:T(8,128)(2,1)S(1)} fusion(bf16[16,1,48,4096]{3,2,1,0:T(8,128)(2,1)} %bitcast.173, pred[16,48]{1,0:T(8,128)(4,1)S(1)} %gt.11), kind=kLoop, calls=%fused_computation.9 | loop fusion | flops 3145728 | bytes 12583680 | tf_op jit(solution)/shard_map/jit(_where)/select_n | solution.py:188
  25.6 80.6 %all_to_all.29 = bf16[16,1,48,4096]{3,2,1,0:T(8,128)(2,1)S(1)} all-to-all(bf16[16,1,48,4096]{3,2,1,0:T(8,128)(2,1)S(1)} %broadcast_select_fusion), channel_id=1, replica_groups=mesh['ep'=16,'tp'=8] {'ep'}, dimensions={0} | all-to-all | bytes 12582912 | tf_op jit(solution)/shard_map/all_to_all | solution.py:192
  106.1 2.6 copy-done.2
  108.7 1.8 fusion.16
  110.5 14.1 %convolution_bitcast_fusion = f32[16,1,48,4096]{3,2,0,1:T(8,128)} fusion(bf16[1,128,4096]{2,1,0:T(8,128)(2,1)S(1)} %copy-done, bf16[16,1,48,4096]{3,2,1,0:T(8,128)(2,1)} %copy-done.2, bf16[1,4096,128]{2,1,0:T(8,128)(2,1)} %param.36, f32[16,1,48,128]{3,2,0,1:T(8,128)S(1)} %fusion.16), kind=kOutput, calls=%fused_computation.4 | convolution fusion | flops 1611202560 | bytes 21364736 | tf_op jit(solution)/shard_map/secf,efd->secd/dot_general | solution.py:199
  124.7 2.2 fusion.4
  127.0 3.6 %convolution_convert_fusion = bf16[256,512]{1,0:T(8,128)(2,1)S(1)} fusion(bf16[4096,512]{1,0:T(8,128)(2,1)} %param.24, bf16[256,4096]{1,0:T(8,128)(2,1)S(1)} %copy-done.3, f32[4096]{0:T(1024)S(1)} %copy-done.12, f32[256]{0:T(256)S(1)} %add_rsqrt_fusion.1), kind=kOutput, calls=%fused_computation.33 | convolution fusion | flops 1078067200 | bytes 6571008 | tf_op jit(solution)/shard_map/dot_general | solution.py:145
  131.2 2.8 %collective-permute-start = (bf16[3,512]{1,0:T(4,128)(2,1)}, bf16[3,512]{1,0:T(4,128)(2,1)}, u32[]{:S(2)}, u32[]{:S(2)}) collective-permute-start(bf16[3,512]{1,0:T(4,128)(2,1)} %slice.437), channel_id=1, source_target_pairs={{0,8},{8,16},{16,24},{24,32},{32,40},{40,48},{48,56},{56,64},{64,7... | collective-permute-start | bytes 9224 | tf_op jit(solution)/shard_map/ppermute | solution.py:36
  135.9 4.9 %fusion.32 = f32[256,4096]{1,0:T(8,128)} fusion(bf16[128,4096]{1,0:T(8,128)(2,1)} %param.40, bf16[256,4096]{1,0:T(8,128)(2,1)S(1)} %fusion.9, bf16[4096,128]{1,0:T(8,128)(2,1)} %param.39, f32[256,128]{1,0:T(8,128)S(1)} %fusion.119), kind=kOutput, calls=%fused_computation.39 | convolution fusion | flops 537067520 | bytes 8519680 | tf_op jit(solution)/shard_map/dot_general | solution.py:212
  140.9 1.0 add_convert_fusion
  148.6 1.7 pad.129
  152.0 1.2 pad.128
  153.2 1.6 pad.113
  154.9 1.0 pad_maximum_fusion.2
  155.9 1.7 pad.112
  159.0 5.0 %all-to-all-start = ((f32[16,2,512]{2,1,0:T(2,128)}), f32[16,2,512]{2,1,0:T(2,128)S(1)}, u32[]{:S(2)}, u32[]{:S(2)}) async-start(f32[16,2,512]{2,1,0:T(2,128)} %broadcast_in_dim.44), calls=%async_computation | async-start | bytes 131072 | tf_op jit(solution)/shard_map/all_to_all | solution.py:41
  164.0 6.5 %all-to-all-done = f32[16,2,512]{2,1,0:T(2,128)S(1)} async-done(((f32[16,2,512]{2,1,0:T(2,128)}), f32[16,2,512]{2,1,0:T(2,128)S(1)}, u32[]{:S(2)}, u32[]{:S(2)}) %all-to-all-start) | async-done | bytes 65568 | tf_op jit(solution)/shard_map/all_to_all | solution.py:41
  170.9 8.6 %fusion.59 = f32[256,4096]{1,0:T(8,128)} fusion(bf16[512,4096]{1,0:T(8,128)(2,1)} %param.29, bf16[4096,512]{1,0:T(8,128)(2,1)} %param.23, bf16[256,4096]{1,0:T(8,128)(2,1)S(1)} %copy-done.4, f32[4096]{0:T(1024)S(1)} %copy-done.12, f32[256]{0:T(256)S(1)} %copy-done.21, f32[256,512]{1,0:T(8,128)S(1)} %pad.128, f32[256,512]{1,0:T(8,128)S(1)} %copy-done.6, ...), kind=kOutput, calls=%fused_computation.55 | convolution fusion | flops 2153512960 | bytes 16796672 | tf_op jit(solution)/shard_map/dot_general | solution.py:178
  179.5 7.7 %pad_maximum_fusion = f32[256,8192]{1,0:T(8,128)} fusion(f32[256,4096]{1,0:T(8,128)} %fusion.32, f32[256,4096]{1,0:T(8,128)} %fusion.59), kind=kLoop, calls=%fused_computation.3 | loop fusion | flops 2097152 | bytes 16777216 | tf_op jit(solution)/shard_map/concatenate | solution.py:86
  188.2 7.5 %reduce-scatter.5.cloned.1.call-done = f32[16,1,48,512]{3,2,0,1:T(8,128)} async-done(((f32[16,1,48,4096]{3,2,0,1:T(8,128)}), f32[16,1,48,512]{3,2,0,1:T(8,128)}) %reduce-scatter.5.cloned.1.call-update) | async-done | bytes 1572880 | tf_op jit(solution)/shard_map/reduce_scatter | solution.py:198
  195.7 1.5 constant_dynamic-slice_fusion.1
  197.3 1.2 collective-permute-start.1
  198.5 2.4 collective-permute-start.2
  200.9 2.2 collective-permute-start.3
  203.1 1.3 collective-permute-start.4
  204.4 1.0 collective-permute-start.5
  207.2 1.3 collective-permute-start.6
  208.6 3.2 %collective-permute-start.7 = (f32[1,1,48,512]{3,2,1,0:T(8,128)S(1)}, f32[1,1,48,512]{3,2,1,0:T(8,128)S(1)}, u32[]{:S(2)}, u32[]{:S(2)}) collective-permute-start(f32[1,1,48,512]{3,2,1,0:T(8,128)S(1)} %get-tuple-element.13), channel_id=1, source_target_pairs={{0,56},{8,64},{16,72},{24,80},{32,88},{40,96},{48,104},{56,112},{6... | collective-permute-start | bytes 294920 | tf_op jit(solution)/shard_map/ppermute | solution.py:28
  211.8 1.7 collective-permute-start.8
  213.5 2.4 collective-permute-start.9
  215.9 2.6 collective-permute-start.10
  218.5 3.0 %collective-permute-start.11 = (f32[1,1,48,512]{3,2,1,0:T(8,128)S(1)}, f32[1,1,48,512]{3,2,1,0:T(8,128)S(1)}, u32[]{:S(2)}, u32[]{:S(2)}) collective-permute-start(f32[1,1,48,512]{3,2,1,0:T(8,128)S(1)} %get-tuple-element.9), channel_id=1, source_target_pairs={{0,88},{8,96},{16,104},{24,112},{32,120},{40,0},{48,8},{56,16},{64... | collective-permute-start | bytes 294920 | tf_op jit(solution)/shard_map/ppermute | solution.py:28
  221.5 2.1 collective-permute-start.12
  223.6 1.4 collective-permute-start.13
  225.0 1.6 collective-permute-start.14
  226.7 1.1 collective-permute-start.15
  228.8 1.3 collective-permute-done.14
  230.1 1.1 collective-permute-done.15
  231.3 1.2 copy-done.7
  232.4 2.1 gather_fusion.1
  234.5 1.6 gather_fusion.2
  236.8 1.3 multiply_reduce_fusion
  238.1 19.1 %all_to_all.30 = f32[8,32,512]{2,1,0:T(8,128)S(1)} all-to-all(f32[8,32,512]{2,1,0:T(8,128)S(1)} %bitcast.176), channel_id=1, replica_groups=mesh['ep'=16,'tp'=8] {'tp'}, dimensions={0} | all-to-all | bytes 1048576 | tf_op jit(solution)/shard_map/all_to_all | solution.py:214
  257.4 1.5 multiply_reduce_fusion.1
  (265 shorter events, 21.1 us)
Async XLA Ops:
  7.2 103.3 %copy-start = (bf16[1,128,4096]{2,1,0:T(8,128)(2,1)S(1)}, bf16[1,128,4096]{2,1,0:T(8,128)(2,1)}, u32[]{:S(2)}) copy-start(bf16[1,128,4096]{2,1,0:T(8,128)(2,1)} %param.37) | copy-start | bytes 3145732
  7.2 6.5 %copy-start.9 = (f32[4096]{0:T(1024)S(1)}, f32[4096]{0:T(1024)}, u32[]{:S(2)}) copy-start(f32[4096]{0:T(1024)} %param.32) | copy-start | bytes 49156
  7.2 188.6 %reduce-scatter.5.cloned.1.call-start = ((), (), s32[]{:S(2)}) async-start(), calls=%async_computation.6 | async-start | bytes 14155776 | tf_op jit(solution)/shard_map/reduce_scatter | solution.py:198
  25.5 83.2 %copy-start.24 = (bf16[1,4096,128]{2,1,0:T(8,128)(2,1)S(1)}, bf16[1,4096,128]{2,1,0:T(8,128)(2,1)}, u32[]{:S(2)}) copy-start(bf16[1,4096,128]{2,1,0:T(8,128)(2,1)} %param.35) | copy-start | bytes 3145732
  106.1 2.6 copy-start.2
  124.7 2.3 copy-start.12
  124.7 2.3 copy-start.3
  126.9 3.6 %copy-start.20 = (f32[256]{0:T(256)}, f32[256]{0:T(256)S(1)}, u32[]{:S(2)}) copy-start(f32[256]{0:T(256)S(1)} %add_rsqrt_fusion.1) | copy-start | bytes 3076
  127.0 7.0 %copy-start.23 = (f32[512]{0:T(512)S(1)}, f32[512]{0:T(512)}, u32[]{:S(2)}) copy-start(f32[512]{0:T(512)} %param.28) | copy-start | bytes 6148
  127.0 7.6 %copy-start.18 = (f32[4,512]{1,0:T(4,128)S(1)}, f32[4,512]{1,0:T(4,128)}, u32[]{:S(2)}) copy-start(f32[4,512]{1,0:T(4,128)} %param.25) | copy-start | bytes 24580
  127.0 8.2 %copy-start.8 = (bf16[4096,128]{1,0:T(8,128)(2,1)S(1)}, bf16[4096,128]{1,0:T(8,128)(2,1)}, u32[]{:S(2)}) copy-start(bf16[4096,128]{1,0:T(8,128)(2,1)} %param.38) | copy-start | bytes 3145732
  131.2 9.7 %collective-permute-start = (bf16[3,512]{1,0:T(4,128)(2,1)}, bf16[3,512]{1,0:T(4,128)(2,1)}, u32[]{:S(2)}, u32[]{:S(2)}) collective-permute-start(bf16[3,512]{1,0:T(4,128)(2,1)} %slice.437), channel_id=1, source_target_pairs={{0,8},{8,16},{16,24},{24,32},{32,40},{40,48},{48,56},{56,64},{64,7... | collective-permute-start | bytes 9224 | tf_op jit(solution)/shard_map/ppermute | solution.py:36
  135.8 5.0 %copy-start.14 = (f32[1,512]{1,0:T(1,128)S(1)}, f32[1,512]{1,0:T(1,128)}, u32[]{:S(2)}) copy-start(f32[1,512]{1,0:T(1,128)} %get-tuple-element.58) | copy-start | bytes 6148
  135.8 5.0 %copy-start.15 = (f32[1,512]{1,0:T(1,128)S(1)}, f32[1,512]{1,0:T(1,128)}, u32[]{:S(2)}) copy-start(f32[1,512]{1,0:T(1,128)} %get-tuple-element.59) | copy-start | bytes 6148
  135.9 5.0 %copy-start.16 = (f32[1,512]{1,0:T(1,128)S(1)}, f32[1,512]{1,0:T(1,128)}, u32[]{:S(2)}) copy-start(f32[1,512]{1,0:T(1,128)} %get-tuple-element.60) | copy-start | bytes 6148
  135.9 5.0 %copy-start.17 = (f32[1,512]{1,0:T(1,128)S(1)}, f32[1,512]{1,0:T(1,128)}, u32[]{:S(2)}) copy-start(f32[1,512]{1,0:T(1,128)} %get-tuple-element.61) | copy-start | bytes 6148
  135.9 6.1 %copy-start.25 = (bf16[2,256,256]{2,1,0:T(8,128)(2,1)S(1)}, bf16[2,256,256]{2,1,0:T(8,128)(2,1)}, u32[]{:S(2)}) copy-start(bf16[2,256,256]{2,1,0:T(8,128)(2,1)} %param.27) | copy-start | bytes 786436
  140.9 1.6 copy-start.26
  142.5 0.6 copy-start.19
  151.3 6.3 %copy-start.6 = (f32[256,512]{1,0:T(8,128)S(1)}, f32[256,512]{1,0:T(8,128)}, u32[]{:S(2)}) copy-start(f32[256,512]{1,0:T(8,128)} %pad.129) | copy-start | bytes 1572868
  151.3 19.6 %copy-start.4 = (bf16[256,4096]{1,0:T(8,128)(2,1)S(1)}, bf16[256,4096]{1,0:T(8,128)(2,1)}, u32[]{:S(2)}) copy-start(bf16[256,4096]{1,0:T(8,128)(2,1)} %param.21) | copy-start | bytes 6291460
  151.3 19.6 %copy-start.21 = (f32[256]{0:T(256)S(1)}, f32[256]{0:T(256)}, u32[]{:S(2)}) copy-start(f32[256]{0:T(256)} %copy-done.20) | copy-start | bytes 3076
  159.0 11.5 %all-to-all-start = ((f32[16,2,512]{2,1,0:T(2,128)}), f32[16,2,512]{2,1,0:T(2,128)S(1)}, u32[]{:S(2)}, u32[]{:S(2)}) async-start(f32[16,2,512]{2,1,0:T(2,128)} %broadcast_in_dim.44), calls=%async_computation | async-start | bytes 131072 | tf_op jit(solution)/shard_map/all_to_all | solution.py:41
  164.0 93.4 %reduce-scatter.3.cloned.1.call-start = ((), (), s32[]{:S(2)}) async-start(), calls=%async_computation.5 | async-start | bytes 9437184 | tf_op jit(solution)/shard_map/reduce_scatter | solution.py:87
  187.3 0.7 copy-start.22
  197.3 9.9 %collective-permute-start.1 = (f32[1,1,48,512]{3,2,1,0:T(8,128)S(1)}, f32[1,1,48,512]{3,2,1,0:T(8,128)S(1)}, u32[]{:S(2)}, u32[]{:S(2)}) collective-permute-start(f32[1,1,48,512]{3,2,1,0:T(8,128)S(1)} %get-tuple-element.19), channel_id=1, source_target_pairs={{0,8},{8,16},{16,24},{24,32},{32,40},{40,48},{48,56},{56,64},{64,7... | collective-permute-start | bytes 294920 | tf_op jit(solution)/shard_map/ppermute | solution.py:28
  198.5 10.0 %collective-permute-start.2 = (f32[1,1,48,512]{3,2,1,0:T(8,128)S(1)}, f32[1,1,48,512]{3,2,1,0:T(8,128)S(1)}, u32[]{:S(2)}, u32[]{:S(2)}) collective-permute-start(f32[1,1,48,512]{3,2,1,0:T(8,128)S(1)} %get-tuple-element.18), channel_id=1, source_target_pairs={{0,16},{8,24},{16,32},{24,40},{32,48},{40,56},{48,64},{56,72},{64,... | collective-permute-start | bytes 294920 | tf_op jit(solution)/shard_map/ppermute | solution.py:28
  200.9 10.9 %collective-permute-start.3 = (f32[1,1,48,512]{3,2,1,0:T(8,128)S(1)}, f32[1,1,48,512]{3,2,1,0:T(8,128)S(1)}, u32[]{:S(2)}, u32[]{:S(2)}) collective-permute-start(f32[1,1,48,512]{3,2,1,0:T(8,128)S(1)} %get-tuple-element.17), channel_id=1, source_target_pairs={{0,24},{8,32},{16,40},{24,48},{32,56},{40,64},{48,72},{56,80},{64,... | collective-permute-start | bytes 294920 | tf_op jit(solution)/shard_map/ppermute | solution.py:28
  203.1 10.4 %collective-permute-start.4 = (f32[1,1,48,512]{3,2,1,0:T(8,128)S(1)}, f32[1,1,48,512]{3,2,1,0:T(8,128)S(1)}, u32[]{:S(2)}, u32[]{:S(2)}) collective-permute-start(f32[1,1,48,512]{3,2,1,0:T(8,128)S(1)} %get-tuple-element.16), channel_id=1, source_target_pairs={{0,32},{8,40},{16,48},{24,56},{32,64},{40,72},{48,80},{56,88},{64,... | collective-permute-start | bytes 294920 | tf_op jit(solution)/shard_map/ppermute | solution.py:28
  204.4 11.5 %collective-permute-start.5 = (f32[1,1,48,512]{3,2,1,0:T(8,128)S(1)}, f32[1,1,48,512]{3,2,1,0:T(8,128)S(1)}, u32[]{:S(2)}, u32[]{:S(2)}) collective-permute-start(f32[1,1,48,512]{3,2,1,0:T(8,128)S(1)} %get-tuple-element.15), channel_id=1, source_target_pairs={{0,40},{8,48},{16,56},{24,64},{32,72},{40,80},{48,88},{56,96},{64,... | collective-permute-start | bytes 294920 | tf_op jit(solution)/shard_map/ppermute | solution.py:28
  207.2 11.3 %collective-permute-start.6 = (f32[1,1,48,512]{3,2,1,0:T(8,128)S(1)}, f32[1,1,48,512]{3,2,1,0:T(8,128)S(1)}, u32[]{:S(2)}, u32[]{:S(2)}) collective-permute-start(f32[1,1,48,512]{3,2,1,0:T(8,128)S(1)} %get-tuple-element.14), channel_id=1, source_target_pairs={{0,48},{8,56},{16,64},{24,72},{32,80},{40,88},{48,96},{56,104},{64... | collective-permute-start | bytes 294920 | tf_op jit(solution)/shard_map/ppermute | solution.py:28
  208.6 13.0 %collective-permute-start.7 = (f32[1,1,48,512]{3,2,1,0:T(8,128)S(1)}, f32[1,1,48,512]{3,2,1,0:T(8,128)S(1)}, u32[]{:S(2)}, u32[]{:S(2)}) collective-permute-start(f32[1,1,48,512]{3,2,1,0:T(8,128)S(1)} %get-tuple-element.13), channel_id=1, source_target_pairs={{0,56},{8,64},{16,72},{24,80},{32,88},{40,96},{48,104},{56,112},{6... | collective-permute-start | bytes 294920 | tf_op jit(solution)/shard_map/ppermute | solution.py:28
  211.8 11.8 %collective-permute-start.8 = (f32[1,1,48,512]{3,2,1,0:T(8,128)S(1)}, f32[1,1,48,512]{3,2,1,0:T(8,128)S(1)}, u32[]{:S(2)}, u32[]{:S(2)}) collective-permute-start(f32[1,1,48,512]{3,2,1,0:T(8,128)S(1)} %get-tuple-element.12), channel_id=1, source_target_pairs={{0,64},{8,72},{16,80},{24,88},{32,96},{40,104},{48,112},{56,120},{... | collective-permute-start | bytes 294920 | tf_op jit(solution)/shard_map/ppermute | solution.py:28
  213.5 11.5 %collective-permute-start.9 = (f32[1,1,48,512]{3,2,1,0:T(8,128)S(1)}, f32[1,1,48,512]{3,2,1,0:T(8,128)S(1)}, u32[]{:S(2)}, u32[]{:S(2)}) collective-permute-start(f32[1,1,48,512]{3,2,1,0:T(8,128)S(1)} %get-tuple-element.11), channel_id=1, source_target_pairs={{0,72},{8,80},{16,88},{24,96},{32,104},{40,112},{48,120},{56,0},{6... | collective-permute-start | bytes 294920 | tf_op jit(solution)/shard_map/ppermute | solution.py:28
  215.9 10.8 %collective-permute-start.10 = (f32[1,1,48,512]{3,2,1,0:T(8,128)S(1)}, f32[1,1,48,512]{3,2,1,0:T(8,128)S(1)}, u32[]{:S(2)}, u32[]{:S(2)}) collective-permute-start(f32[1,1,48,512]{3,2,1,0:T(8,128)S(1)} %get-tuple-element.10), channel_id=1, source_target_pairs={{0,80},{8,88},{16,96},{24,104},{32,112},{40,120},{48,0},{56,8},{64... | collective-permute-start | bytes 294920 | tf_op jit(solution)/shard_map/ppermute | solution.py:28
  218.5 9.3 %collective-permute-start.11 = (f32[1,1,48,512]{3,2,1,0:T(8,128)S(1)}, f32[1,1,48,512]{3,2,1,0:T(8,128)S(1)}, u32[]{:S(2)}, u32[]{:S(2)}) collective-permute-start(f32[1,1,48,512]{3,2,1,0:T(8,128)S(1)} %get-tuple-element.9), channel_id=1, source_target_pairs={{0,88},{8,96},{16,104},{24,112},{32,120},{40,0},{48,8},{56,16},{64... | collective-permute-start | bytes 294920 | tf_op jit(solution)/shard_map/ppermute | solution.py:28
  221.5 6.7 %collective-permute-start.12 = (f32[1,1,48,512]{3,2,1,0:T(8,128)S(1)}, f32[1,1,48,512]{3,2,1,0:T(8,128)S(1)}, u32[]{:S(2)}, u32[]{:S(2)}) collective-permute-start(f32[1,1,48,512]{3,2,1,0:T(8,128)S(1)} %get-tuple-element.8), channel_id=1, source_target_pairs={{0,96},{8,104},{16,112},{24,120},{32,0},{40,8},{48,16},{56,24},{64... | collective-permute-start | bytes 294920 | tf_op jit(solution)/shard_map/ppermute | solution.py:28
  223.6 5.1 %collective-permute-start.13 = (f32[1,1,48,512]{3,2,1,0:T(8,128)S(1)}, f32[1,1,48,512]{3,2,1,0:T(8,128)S(1)}, u32[]{:S(2)}, u32[]{:S(2)}) collective-permute-start(f32[1,1,48,512]{3,2,1,0:T(8,128)S(1)} %get-tuple-element.7), channel_id=1, source_target_pairs={{0,104},{8,112},{16,120},{24,0},{32,8},{40,16},{48,24},{56,32},{64... | collective-permute-start | bytes 294920 | tf_op jit(solution)/shard_map/ppermute | solution.py:28
  225.0 5.0 %collective-permute-start.14 = (f32[1,1,48,512]{3,2,1,0:T(8,128)S(1)}, f32[1,1,48,512]{3,2,1,0:T(8,128)S(1)}, u32[]{:S(2)}, u32[]{:S(2)}) collective-permute-start(f32[1,1,48,512]{3,2,1,0:T(8,128)S(1)} %get-tuple-element.6), channel_id=1, source_target_pairs={{0,112},{8,120},{16,0},{24,8},{32,16},{40,24},{48,32},{56,40},{64,... | collective-permute-start | bytes 294920 | tf_op jit(solution)/shard_map/ppermute | solution.py:28
  226.7 4.6 %collective-permute-start.15 = (f32[1,1,48,512]{3,2,0,1:T(8,128)S(1)}, f32[1,1,48,512]{3,2,0,1:T(8,128)S(1)}, u32[]{:S(2)}, u32[]{:S(2)}) collective-permute-start(f32[1,1,48,512]{3,2,0,1:T(8,128)S(1)} %constant_dynamic-slice_fusion), channel_id=1, source_target_pairs={{0,120},{8,0},{16,8},{24,16},{32,24},{40,32},{48,40},{56,48},{64,5... | collective-permute-start | bytes 294920 | tf_op jit(solution)/shard_map/ppermute | solution.py:28
  227.8 6.7 %copy-start.13 = (s32[1024]{0:T(1024)S(1)}, s32[1024]{0:T(1024)}, u32[]{:S(2)}) copy-start(s32[1024]{0:T(1024)} %get-tuple-element.70) | copy-start | bytes 12292
  231.3 1.2 copy-start.7
  238.1 20.8 %copy-start.10 = (f32[4096]{0:T(1024)S(1)}, f32[4096]{0:T(1024)}, u32[]{:S(2)}) copy-start(f32[4096]{0:T(1024)} %param.41) | copy-start | bytes 49156
  238.1 20.8 %copy-start.11 = (f32[4096]{0:T(1024)S(1)}, f32[4096]{0:T(1024)}, u32[]{:S(2)}) copy-start(f32[4096]{0:T(1024)} %param.30) | copy-start | bytes 49156
  257.3 2.6 copy-start.1
  257.3 1.6 copy-start.5
Sparse Core Ops, SparseCore 0:
  124.8 70.9 reduce-scatter.4
  198.1 52.0 reduce-scatter.2
